TPU v7x, 32 devices: a whole 2x2x4 slice. The times are simulated.
32 devices in a mesh: grp: 2 (over y), sp: 4 (over z), tp: 4 (over x, core).
Axes of the slice: x: 2, y: 2, z: 4, core: 2. Of those that a mesh axis runs over, the one named last changes fastest.
Arguments:
- target: bfloat16 [2048, 2048], P(('grp', 'sp', 'tp')), parts along dimension 0, may hold values from -20 to 20
- source: bfloat16 [4096, 2048], P(('grp', 'sp')), parts along dimension 0, may hold values from -20 to 20
- source_gain: float32 [2048], replicated, may hold values from 0.1 to 1.9
- query_gain: float32 [2, 2048], replicated, may hold values from 0.1 to 1.9
- out_gain: float32 [2, 2048], replicated, may hold values from 0.1 to 1.9
- query_weight: bfloat16 [2, 2048, 2048], P(None, None, 'tp'), may hold values from -1 to 1
- key_weight: bfloat16 [2, 2048, 512], P(None, None, 'tp'), may hold values from -1 to 1
- value_weight: bfloat16 [2, 2048, 512], P(None, None, 'tp'), may hold values from -0.125 to 0.125
- out_weight: bfloat16 [2, 2048, 2048], P(None, 'tp'), may hold values from -0.125 to 0.125
Outputs:
- result: bfloat16 [2048, 2048], P(('grp', 'sp', 'tp')), parts along dimension 0
There are 2 independent parts, one for each index of `grp`. A program takes and returns all parts, laid end to end along the dimension named above; an argument that names none is the same for every part. Nothing has to cross between parts.
All inputs are finite; a program needn't handle non-finite values.
Results may differ from a plain program's by a relative error of at most 0.024.
Values may be sent and summed in bfloat16 or wider, within the bound.
A program may use at most 64 MiB of HBM per device.

v0:
```python
import jax
import jax.numpy as jnp
from jax import lax
from jax.sharding import PartitionSpec as P

HD = 256
QH = 8
KVH = 2
LAYERS = 2


EPSILON = 1e-06


def swapped(value, axis, distance):
    mask = 2**distance
    pairs = [(source, source ^ mask) for source in range(lax.axis_size(axis))]
    return lax.ppermute(value, axis, pairs)


def rms_scaled(matrix_rows, gain_row):
    values = matrix_rows.astype(jnp.float32)
    inverse = lax.rsqrt(jnp.mean(values * values, axis=-1, keepdims=True) + EPSILON)
    return values * inverse * gain_row


def group_rounds(holding, bit_count, position):
    for bit_number in range(bit_count):
        my_bit = position >> bit_number & 1
        if holding.shape[0] > 1:
            halves = holding.reshape((holding.shape[0] // 2, 2) + holding.shape[1:])
            kept_part = lax.dynamic_index_in_dim(halves, my_bit, 1, False)
            outgoing = lax.dynamic_index_in_dim(halves, 1 - my_bit, 1, False)
        else:
            kept_part = holding
            outgoing = holding
        arrived = swapped(outgoing, "tp", bit_number)
        holding = jnp.where(
            my_bit == 0,
            jnp.concatenate([kept_part, arrived], 1),
            jnp.concatenate([arrived, kept_part], 1),
        )
    return holding


def spread_heads(factor, piece_index, piece_width):
    columns = jnp.repeat(factor, HD, axis=1)
    pieces = columns.reshape(factor.shape[0], columns.shape[1] // piece_width, piece_width)
    return jnp.take(pieces, piece_index, axis=1)


def merge_partials(weighted, row_peak, row_total, bit_count, position):
    piece_width = weighted.shape[2]
    piece_index = jnp.arange(weighted.shape[1], dtype=jnp.int32)
    for bit_number in range(bit_count):
        my_bit = position >> bit_number & 1
        halves = weighted.reshape(weighted.shape[0], weighted.shape[1] // 2, 2, piece_width)
        kept_part = lax.dynamic_index_in_dim(halves, my_bit, 2, False)
        outgoing = lax.dynamic_index_in_dim(halves, 1 - my_bit, 2, False)
        piece_index = lax.dynamic_index_in_dim(piece_index.reshape(-1, 2), my_bit, 1, False)
        far_weighted, far_peak, far_total = (
            swapped(outgoing.astype(jnp.bfloat16), "tp", bit_number).astype(outgoing.dtype),
            swapped(row_peak.astype(jnp.bfloat16), "tp", bit_number).astype(row_peak.dtype),
            swapped(row_total.astype(jnp.bfloat16), "tp", bit_number).astype(row_total.dtype),
        )
        new_peak = jnp.maximum(row_peak, far_peak)
        near_factor = jnp.exp(row_peak - new_peak)
        far_factor = jnp.exp(far_peak - new_peak)
        row_total = row_total * near_factor + far_total * far_factor
        weighted = kept_part * spread_heads(
            near_factor, piece_index, piece_width
        ) + far_weighted * spread_heads(far_factor, piece_index, piece_width)
        row_peak = new_peak
    return (weighted, row_total, piece_index)


def attend(carried, key_rows, value_rows, grouped, score_scale):
    row_peak, row_total, weighted = carried
    scores = (
        jnp.einsum("rhd,nd->rhn", grouped, key_rows, preferred_element_type=jnp.float32)
        * score_scale
    )
    new_peak = jnp.maximum(row_peak, jnp.max(scores, axis=2))
    weights = jnp.exp(scores - new_peak[:, :, None])
    row_total = jnp.sum(weights, axis=2)
    weighted = jnp.einsum(
        "rhn,nd->rhd", weights.astype(jnp.bfloat16), value_rows, preferred_element_type=jnp.float32
    )
    return (new_peak, row_total, weighted)


def body(
    target,
    source,
    source_gain,
    query_gain,
    out_gain,
    query_weight,
    key_weight,
    value_weight,
    out_weight,
):
    tp_devices = lax.axis_size("tp")
    group_size = tp_devices // KVH
    bit_count = group_size.bit_length() - 1
    position = lax.axis_index("tp") % group_size
    score_scale = HD ** (-0.5)
    heads_here = QH // KVH
    matrices = 2 * LAYERS
    slices = key_weight.shape[2]
    block_rows = source.shape[0] // group_size
    normed_source = rms_scaled(source, source_gain).astype(jnp.bfloat16)
    joined = jnp.concatenate(
        [
            matrix[layer_index]
            for layer_index in range(LAYERS)
            for matrix in (key_weight, value_weight)
        ],
        axis=1,
    )
    key_slices = jnp.dot(normed_source, joined, preferred_element_type=jnp.float32).astype(
        jnp.bfloat16
    )
    holding = group_rounds(
        key_slices.reshape(group_size, 1, block_rows, matrices, slices), bit_count, position
    )
    local_keys = jnp.transpose(holding[0], (2, 1, 0, 3)).reshape(matrices, block_rows, HD)
    residual = target
    stored = None
    for layer_index in range(LAYERS):
        normed = rms_scaled(residual, query_gain[layer_index]).astype(jnp.bfloat16)
        layer_weight = query_weight[layer_index]
        queries = jnp.dot(
            lax.all_gather(normed, "tp", axis=0, tiled=True),
            layer_weight,
            preferred_element_type=jnp.float32,
        ).astype(jnp.bfloat16)
        rows_all = queries.shape[0]
        gathered = group_rounds(queries[None, None], bit_count, position)[0]
        grouped = jnp.transpose(gathered, (1, 0, 2)).reshape(rows_all, heads_here, HD)
        start_state = (
            jnp.full((rows_all, heads_here), -1e30, jnp.float32),
            jnp.zeros((rows_all, heads_here), jnp.float32),
            jnp.zeros((rows_all, heads_here, HD), jnp.float32),
        )
        if layer_index == 0:
            empty_rows = jnp.zeros(
                (lax.axis_size("sp") * block_rows, matrices - 2, HD), jnp.bfloat16
            )
            later_keys = jnp.transpose(local_keys[2:], (1, 0, 2))
            updated = attend(
                (start_state + (empty_rows,))[:3],
                lax.all_gather(local_keys[0], "sp", axis=0, tiled=True),
                lax.all_gather(local_keys[1], "sp", axis=0, tiled=True),
                grouped,
                score_scale,
            )
            kept_rows = lax.all_gather(later_keys, "sp", axis=0, tiled=True)
            row_peak, row_total, weighted, stored = updated + (kept_rows,)
        else:
            row_peak, row_total, weighted = attend(
                start_state,
                stored[:, 2 * layer_index - 2],
                stored[:, 2 * layer_index - 1],
                grouped,
                score_scale,
            )
        piece_width = heads_here * HD // group_size
        merged, row_total, piece_index = merge_partials(
            weighted.reshape(rows_all, group_size, piece_width),
            row_peak,
            row_total,
            bit_count,
            position,
        )
        attended = (merged[:, 0] / spread_heads(row_total, piece_index, piece_width)[:, 0]).astype(
            jnp.bfloat16
        )
        out_layer = out_weight[layer_index]
        summed_rows = lax.psum_scatter(
            jnp.dot(attended, out_layer, preferred_element_type=jnp.float32).astype(jnp.bfloat16),
            "tp",
            scatter_dimension=0,
            tiled=True,
        ).astype(jnp.float32)
        residual = (
            residual.astype(jnp.float32) + rms_scaled(summed_rows, out_gain[layer_index])
        ).astype(jnp.bfloat16)
    return residual


def solution(mesh):
    in_specs = (
        P(("grp", "sp", "tp"), None),
        P(("grp", "sp"), None),
        P(),
        P(),
        P(),
        P(None, None, "tp"),
        P(None, None, "tp"),
        P(None, None, "tp"),
        P(None, "tp", None),
    )
    out_specs = P(("grp", "sp", "tp"), None)
    return jax.shard_map(body, mesh=mesh, in_specs=in_specs, out_specs=out_specs, check_vma=False)
```

profile of v0, /device:TPU:0, one launch (start us, length us, event | category | flops | bytes accessed | tf_op | source)
XLA Modules:
  0.0 189.7 jit_solution(303224144333175223)
XLA Ops:
  6.5 0.9 fusion.100
  7.4 1.1 fusion.51
  8.6 1.8 fusion.53
  10.4 2.7 %slice_bitcast_fusion.6 = (bf16[2048,128]{1,0:T(8,128)(2,1)S(1)}, bf16[2048,128]{1,0:T(8,128)(2,1)}, bf16[2048,128]{1,0:T(8,128)(2,1)}, bf16[2048,128]{1,0:T(8,128)(2,1)}) fusion(bf16[2,2048,128]{2,1,0:T(8,128)(2,1)} %param.18, bf16[2,2048,128]{2,1,0:T(8,128)(2,1)} %param.17), kind=kLoop, calls=%fused_computation.92 | loop fusion | bytes 4194304 | tf_op jit(solution)/shard_map/squeeze | solution.py:115
  13.2 0.5 fusion
  13.7 2.7 %fusion.36 = bf16[512,512]{1,0:T(8,128)(2,1)S(1)} fusion(bf16[2048,128]{1,0:T(8,128)(2,1)} %get-tuple-element.28, bf16[2048,128]{1,0:T(8,128)(2,1)} %get-tuple-element.41, bf16[2048,128]{1,0:T(8,128)(2,1)S(1)} %get-tuple-element.27, bf16[2048,128]{1,0:T(8,128)(2,1)} %get-tuple-element.42, bf16[512,2048]{1,0:T(8,128)(2,1)S(1)} %copy-done.1, ...), kind=kOutput, calls=%fused_computation.41 | convolution fusion | flops 1086586880 | bytes 4728832 | tf_op jit(solution)/shard_map/dot_general | solution.py:121
  16.3 0.1 reshape_reshape.27
  16.5 0.2 constant_dynamic-slice_fusion.2
  16.7 0.6 collective-permute-start.1
  17.3 1.1 collective-permute-done.1
  18.5 0.1 copy.15
  18.7 11.2 %all-gather.4.cloned.1.call-done = bf16[256,2048]{1,0:T(8,128)(2,1)} async-done(((bf16[64,2048]{1,0:T(8,128)(2,1)}), bf16[256,2048]{1,0:T(8,128)(2,1)}) %all-gather.4.cloned.1.call-update) | async-done | bytes 1048592 | tf_op jit(solution)/shard_map/all_gather | solution.py:134
  30.0 2.6 %fusion.41 = bf16[256,512]{1,0:T(8,128)(2,1)S(1)} fusion(bf16[256,2048]{1,0:T(8,128)(2,1)} %all-gather.4.cloned.1.call-done, bf16[2,2048,512]{2,1,0:T(8,128)(2,1)} %param.16), kind=kOutput, calls=%fused_computation.42 | convolution fusion | flops 537001984 | bytes 3407872 | tf_op jit(solution)/shard_map/dot_general | solution.py:133
  32.6 0.3 collective-permute-start
  32.9 16.0 %all_gather.16 = bf16[1024,256]{1,0:T(8,128)(2,1)S(1)} all-gather(bf16[256,256]{1,0:T(8,128)(2,1)S(1)} %bitcast.151), channel_id=1, replica_groups=mesh['grp'=2,'sp'=4,'tp'=4] {'sp'}, dimensions={0}, use_global_device_ids=true | all-gather | bytes 655360 | tf_op jit(solution)/shard_map/all_gather | solution.py:153
  48.9 0.1 copy.17
  49.0 16.1 %all_gather.17 = bf16[1024,256]{0,1:T(8,128)(2,1)S(1)} all-gather(bf16[256,256]{0,1:T(8,128)(2,1)S(1)} %bitcast.152), channel_id=1, replica_groups=mesh['grp'=2,'sp'=4,'tp'=4] {'sp'}, dimensions={0}, use_global_device_ids=true | all-gather | bytes 655360 | tf_op jit(solution)/shard_map/all_gather | solution.py:154
  65.2 0.2 copy.12
  65.4 0.8 multiply_reduce_fusion.1
  66.2 0.9 fusion.3
  67.2 1.0 fusion.9
  68.3 0.5 collective-permute-start.4
  68.8 0.1 collective-permute-start.2
  68.9 0.6 constant_dynamic-slice_fusion
  71.7 1.9 convolution_convert_fusion.1
  73.7 24.6 %reduce-scatter.3.cloned.1.call-done = bf16[64,2048]{1,0:T(8,128)(2,1)} async-done(((bf16[256,2048]{1,0:T(8,128)(2,1)}), bf16[64,2048]{1,0:T(8,128)(2,1)}) %reduce-scatter.3.cloned.1.call-update) | async-done | bytes 262160 | tf_op jit(solution)/shard_map/reduce_scatter | solution.py:180
  98.3 1.1 fusion.47
  99.5 1.2 fusion.55
  100.7 0.8 fusion.57
  101.7 0.7 bitcast_bitcast_fusion
  102.4 0.2 reduce-scatter.5.cloned.1.call-start
  102.7 15.8 %all-gather.6.cloned.1.call-done = bf16[256,2048]{1,0:T(8,128)(2,1)} async-done(((bf16[64,2048]{1,0:T(8,128)(2,1)}), bf16[256,2048]{1,0:T(8,128)(2,1)}) %all-gather.6.cloned.1.call-update) | async-done | bytes 1048592 | tf_op jit(solution)/shard_map/all_gather | solution.py:134
  118.5 2.6 %fusion.44 = bf16[256,512]{1,0:T(8,128)(2,1)S(1)} fusion(bf16[256,2048]{1,0:T(8,128)(2,1)} %all-gather.6.cloned.1.call-done, bf16[2,2048,512]{2,1,0:T(8,128)(2,1)} %param.16), kind=kOutput, calls=%fused_computation.43 | convolution fusion | flops 537001984 | bytes 3407872 | tf_op jit(solution)/shard_map/dot_general | solution.py:133
  121.1 0.3 collective-permute-start.5
  121.4 1.3 collective-permute-done.5
  122.8 0.2 copy.18
  123.0 24.9 %all-gather.8.cloned.1.call-done = bf16[1024,2,256]{2,0,1:T(8,128)(2,1)} async-done(((bf16[256,2,256]{2,0,1:T(8,128)(2,1)}), bf16[1024,2,256]{2,0,1:T(8,128)(2,1)}) %all-gather.8.cloned.1.call-update) | async-done | bytes 1048592 | tf_op jit(solution)/shard_map/all_gather | solution.py:158
  147.9 2.0 %multiply_reduce_fusion = (f32[256,4]{0,1:T(4,128)S(1)}, f32[256,4,1024]{2,0,1:T(8,128)S(1)}) fusion(bf16[256,4,256]{0,2,1:T(8,128)(2,1)S(1)} %bitcast.138, bf16[1024,2,256]{2,0,1:T(8,128)(2,1)} %all-gather.8.cloned.1.call-done), kind=kOutput, calls=%fused_computation.7 | convolution fusion | flops 538967040 | bytes 5246976 | tf_op jit(solution)/shard_map/rhd,nd->rhn/dot_general | solution.py:80
  149.9 0.9 fusion.5
  150.8 1.1 fusion.7
  152.1 0.5 collective-permute-start.8
  152.6 0.1 collective-permute-start.6
  152.7 0.9 collective-permute-done.8
  153.6 0.1 collective-permute-done.6
  154.0 1.8 convolution_convert_fusion
  155.9 24.3 %reduce-scatter.5.cloned.1.call-done = bf16[64,2048]{1,0:T(8,128)(2,1)} async-done(((bf16[256,2048]{1,0:T(8,128)(2,1)}), bf16[64,2048]{1,0:T(8,128)(2,1)}) %reduce-scatter.5.cloned.1.call-update) | async-done | bytes 262160 | tf_op jit(solution)/shard_map/reduce_scatter | solution.py:180
  180.2 1.1 fusion.49
  181.3 1.8 fusion.58
  (60 shorter events, 1.3 us)
Async XLA Ops:
  6.5 6.6 %copy-start.1 = (bf16[512,2048]{1,0:T(8,128)(2,1)S(1)}, bf16[512,2048]{1,0:T(8,128)(2,1)}, u32[]{:S(2)}) copy-start(bf16[512,2048]{1,0:T(8,128)(2,1)} %param.12) | copy-start | bytes 6291460
  6.5 7.1 %copy-start.6 = (f32[2048]{0:T(1024)S(1)}, f32[2048]{0:T(1024)}, u32[]{:S(2)}) copy-start(f32[2048]{0:T(1024)} %param.13) | copy-start | bytes 24580
  6.5 23.4 %all-gather.4.cloned.1.call-start = ((), (), s32[]{:S(2)}) async-start(), calls=%async_computation.2 | async-start | bytes 1310720 | tf_op jit(solution)/shard_map/all_gather | solution.py:134
  10.4 88.0 %reduce-scatter.3.cloned.1.call-start = ((), (), s32[]{:S(2)}) async-start(), calls=%async_computation.3 | async-start | bytes 1310720 | tf_op jit(solution)/shard_map/reduce_scatter | solution.py:180
  16.7 1.7 collective-permute-start.1
  32.6 32.5 %collective-permute-start = (bf16[1,1,256,512]{3,2,1,0:T(8,128)(2,1)S(1)}, bf16[1,1,256,512]{3,2,1,0:T(8,128)(2,1)S(1)}, u32[]{:S(2)}, u32[]{:S(2)}) collective-permute-start(bf16[1,1,256,512]{3,2,1,0:T(8,128)(2,1)S(1)} %bitcast.155), channel_id=1, source_target_pairs={{0,1},{1,0},{2,3},{3,2},{4,5},{5,4},{6,7},{7,6},{8,9},{9,8},{10,11... | collective-permute-start | bytes 786440 | tf_op jit(solution)/shard_map/ppermute | solution.py:18
  67.2 4.6 %copy-start.4 = (bf16[2,512,2048]{2,1,0:T(8,128)(2,1)S(1)}, bf16[2,512,2048]{2,1,0:T(8,128)(2,1)}, u32[]{:S(2)}) copy-start(bf16[2,512,2048]{2,1,0:T(8,128)(2,1)} %param.19) | copy-start | bytes 12582916
  68.2 3.3 %collective-permute-start.3 = (bf16[256,1,512]{0,2,1:T(8,128)(2,1)S(1)}, bf16[256,1,512]{0,2,1:T(8,128)(2,1)S(1)}, u32[]{:S(2)}, u32[]{:S(2)}) collective-permute-start(bf16[256,1,512]{0,2,1:T(8,128)(2,1)S(1)} %fusion.72), channel_id=1, source_target_pairs={{0,1},{1,0},{2,3},{3,2},{4,5},{5,4},{6,7},{7,6},{8,9},{9,8},{10,11... | collective-permute-start | bytes 786440 | tf_op jit(solution)/shard_map/ppermute | solution.py:18
  68.3 3.1 %collective-permute-start.4 = (bf16[256,4]{0,1:T(4,128)(2,1)S(1)}, bf16[256,4]{0,1:T(4,128)(2,1)S(1)}, u32[]{:S(2)}, u32[]{:S(2)}) collective-permute-start(bf16[256,4]{0,1:T(4,128)(2,1)S(1)} %convert_element_type.135), channel_id=1, source_target_pairs={{0,1},{1,0},{2,3},{3,2},{4,5},{5,4},{6,7},{7,6},{8,9},{9,8},{10,11... | collective-permute-start | bytes 6152 | tf_op jit(solution)/shard_map/ppermute | solution.py:18
  68.8 2.6 %collective-permute-start.2 = (bf16[256,4]{0,1:T(4,128)(2,1)S(1)}, bf16[256,4]{0,1:T(4,128)(2,1)S(1)}, u32[]{:S(2)}, u32[]{:S(2)}) collective-permute-start(bf16[256,4]{0,1:T(4,128)(2,1)S(1)} %fusion.91), channel_id=1, source_target_pairs={{0,1},{1,0},{2,3},{3,2},{4,5},{5,4},{6,7},{7,6},{8,9},{9,8},{10,11... | collective-permute-start | bytes 6152 | tf_op jit(solution)/shard_map/ppermute | solution.py:18
  71.6 2.0 %copy-start.3 = (f32[2,2048]{1,0:T(2,128)S(1)}, f32[2,2048]{1,0:T(2,128)}, u32[]{:S(2)}) copy-start(f32[2,2048]{1,0:T(2,128)} %param.15) | copy-start | bytes 49156
  71.6 27.8 %copy-start = (bf16[64,2048]{1,0:T(8,128)(2,1)S(1)}, bf16[64,2048]{1,0:T(8,128)(2,1)}, u32[]{:S(2)}) copy-start(bf16[64,2048]{1,0:T(8,128)(2,1)} %param.11) | copy-start | bytes 786436
  73.6 44.8 %all-gather.6.cloned.1.call-start = ((), (), s32[]{:S(2)}) async-start(), calls=%async_computation.4 | async-start | bytes 1310720 | tf_op jit(solution)/shard_map/all_gather | solution.py:134
  101.6 46.3 %all-gather.8.cloned.1.call-start = ((), (), s32[]{:S(2)}) async-start(), calls=%async_computation.5 | async-start | bytes 1310720 | tf_op jit(solution)/shard_map/all_gather | solution.py:158
  102.4 77.8 %reduce-scatter.5.cloned.1.call-start = ((), (), s32[]{:S(2)}) async-start(), calls=%async_computation.6 | async-start | bytes 1310720 | tf_op jit(solution)/shard_map/reduce_scatter | solution.py:180
  121.1 1.6 collective-permute-start.5
  147.9 2.9 %copy-start.2 = (bf16[1024,2,256]{2,0,1:T(8,128)(2,1)S(1)}, bf16[1024,2,256]{2,0,1:T(8,128)(2,1)}, u32[]{:S(2)}) copy-start(bf16[1024,2,256]{2,0,1:T(8,128)(2,1)} %all-gather.8.cloned.1.call-done) | copy-start | bytes 3145732
  150.8 3.2 %copy-start.5 = (bf16[2,512,2048]{2,1,0:T(8,128)(2,1)S(1)}, bf16[2,512,2048]{2,1,0:T(8,128)(2,1)}, u32[]{:S(2)}) copy-start(bf16[2,512,2048]{2,1,0:T(8,128)(2,1)} %param.19) | copy-start | bytes 12582916
  152.0 1.8 collective-permute-start.7
  152.1 1.5 collective-permute-start.8
  152.6 1.2 collective-permute-start.6
Sparse Core Ops, SparseCore 0:
  10.5 19.4 all-gather.3
  73.7 24.5 reduce-scatter.2
  101.7 16.6 all-gather.5
  119.9 27.9 all-gather.7
  156.0 24.1 reduce-scatter.4
where the time goes:
time: 190 us
  waiting for transfers between devices  105 us (55%)
  blocking collectives  32.1 us (17%)
  matrix products  16.5 us (9%)
  between operations  15.5 us (8%)
  other arithmetic  11.6 us (6%)
  local copies, waits for them, and re-layouts  6.59 us (3%)
  starting transfers between devices  2.78 us (1%)
    reduce_scatter x2, waiting for transfers between devices, body(): lax.psum_scatter(jnp.dot(attended, out_layer, preferred_element_type=jnp....  49 us
    all_gather x2, waiting for transfers between devices, body(): lax.all_gather(normed, 'tp', axis=0, tiled=True)  27 us
    all_gather x1, waiting for transfers between devices, body(): kept_rows = lax.all_gather(later_keys, 'sp', axis=0, tiled=True)  24.9 us
    all_gather x1, blocking collectives, body(): lax.all_gather(local_keys[1], 'sp', axis=0, tiled=True)  16.1 us
    all_gather x1, blocking collectives, body(): lax.all_gather(local_keys[0], 'sp', axis=0, tiled=True)  16 us
    dot_general x2, matrix products, body(): jnp.dot(lax.all_gather(normed, 'tp', axis=0, tiled=True), layer_weight, p...  5.24 us
    reduce_sum x5, other arithmetic, rms_scaled(): jnp.mean(values * values, axis=-1, keepdims=True) + EPSILON  5.04 us
  transfers between devices with their start and end apart: 14, of which 9 were waited for; matrix products, arithmetic and copies ran while one was open for 6% of the time, Pallas kernels for 0%

commit v1 on v0

--- a/solution.py
+++ b/solution.py
@@ -1,6 +1,10 @@
+import functools
+
 import jax
 import jax.numpy as jnp
 from jax import lax
+from jax.experimental import pallas as pl
+from jax.experimental.pallas import tpu as pltpu
 from jax.sharding import PartitionSpec as P
 
 HD = 256
@@ -189,6 +193,407 @@
     return residual
 
 
+CHUNKS = 4
+
+
+def fused_kernel(
+    n,
+    target,
+    source,
+    source_gain,
+    query_gain,
+    out_gain,
+    query_weight,
+    key_weight,
+    value_weight,
+    out_weight,
+    result,
+    res,
+    raw,
+    ns,
+    wkv,
+    wq,
+    wo,
+    kh,
+    xb,
+    sb,
+    rb,
+    pj,
+    qs,
+    ms,
+    ls,
+    acc,
+    load_sem,
+    wload_sem,
+    wsend,
+    wrecv,
+    xsend,
+    xrecv,
+    rsend,
+    rrecv,
+    zsend,
+    zrecv,
+    psend,
+    precv,
+):
+    rows = target.shape[0]
+    block = source.shape[0]
+    half = key_weight.shape[2]
+    wide = target.shape[1] // CHUNKS
+    piece = block // CHUNKS
+    heads = query_weight.shape[2] // HD
+    z = lax.axis_index("sp")
+    me = lax.axis_index("tp")
+    c = me % 2
+    partner = me + 1 - 2 * c
+    across = (me + 2) % 4
+    mesh_ids = pl.DeviceIdType.MESH
+    f32, bf16 = jnp.float32, jnp.bfloat16
+
+    loads = [pltpu.make_async_copy(target, res, load_sem.at[0])]
+    for j in range(CHUNKS):
+        part = pl.ds(j * piece, piece)
+        loads.append(pltpu.make_async_copy(source.at[part], raw.at[part], load_sem.at[1 + j]))
+    kv_loads, q_loads, o_loads = [], [], []
+    for l in range(LAYERS):
+        kv_loads.append(
+            (
+                pltpu.make_async_copy(key_weight.at[l], wkv.at[l, :, pl.ds(0, half)], wload_sem.at[l, 0]),
+                pltpu.make_async_copy(value_weight.at[l], wkv.at[l, :, pl.ds(half, half)], wload_sem.at[l, 1]),
+            )
+        )
+        q_loads.append(pltpu.make_async_copy(query_weight.at[l], wq.at[0, l], wload_sem.at[l, 2]))
+        o_loads.append(pltpu.make_async_copy(out_weight.at[l], wo.at[0, l], wload_sem.at[l, 3]))
+    for copy in loads:
+        copy.start()
+    for l in range(LAYERS):
+        for copy in kv_loads[l]:
+            copy.start()
+    for l in range(LAYERS):
+        q_loads[l].start()
+        o_loads[l].start()
+
+    def to_partner(src, dst, l, which):
+        return pltpu.make_async_remote_copy(
+            src_ref=src,
+            dst_ref=dst,
+            send_sem=wsend.at[l, which],
+            recv_sem=wrecv.at[l, which],
+            device_id={"tp": partner},
+            device_id_type=mesh_ids,
+        )
+
+    q_share = [to_partner(query_weight.at[l], wq.at[1, l], l, 0) for l in range(LAYERS)]
+    o_share = [to_partner(out_weight.at[l], wo.at[1, l], l, 1) for l in range(LAYERS)]
+
+    def gather_copy(l, j):
+        return pltpu.make_async_remote_copy(
+            src_ref=xb.at[l, 0, j],
+            dst_ref=xb.at[l, 1, j],
+            send_sem=xsend.at[l, j],
+            recv_sem=xrecv.at[l, j],
+            device_id={"tp": across},
+            device_id_type=mesh_ids,
+        )
+
+    def scatter_copy(l, j):
+        return pltpu.make_async_remote_copy(
+            src_ref=sb.at[l, j],
+            dst_ref=rb.at[l, j],
+            send_sem=rsend.at[l, j],
+            recv_sem=rrecv.at[l, j],
+            device_id={"tp": across},
+            device_id_type=mesh_ids,
+        )
+
+    signs = (1, -1)
+
+    def inside(index):
+        return jnp.logical_and(index >= 0, index < n)
+
+    def line_copy(l, way, d, kv):
+        ref = kh.at[l, z - signs[way] * (d - 1), c, kv]
+        return pltpu.make_async_remote_copy(
+            src_ref=ref,
+            dst_ref=ref,
+            send_sem=zsend.at[l, way, d, kv],
+            recv_sem=zrecv.at[l, way, d, kv],
+            device_id={"sp": z + signs[way]},
+            device_id_type=mesh_ids,
+        )
+
+    def line_arrival(l, way, d, kv):
+        ref = kh.at[l, z - signs[way] * d, c, kv]
+        return pltpu.make_async_remote_copy(
+            src_ref=ref,
+            dst_ref=ref,
+            send_sem=zsend.at[l, way, d, kv],
+            recv_sem=zrecv.at[l, way, d, kv],
+            device_id={"sp": z - signs[way]},
+            device_id_type=mesh_ids,
+        )
+
+    def pair_copy(l, way, d, kv, side):
+        ref = kh.at[l, z - signs[way] * d, side, kv]
+        return pltpu.make_async_remote_copy(
+            src_ref=ref,
+            dst_ref=ref,
+            send_sem=psend.at[l, way, d, kv],
+            recv_sem=precv.at[l, way, d, kv],
+            device_id={"tp": partner},
+            device_id_type=mesh_ids,
+        )
+
+    def send_own(l):
+        for kv in range(2):
+            for way in range(2):
+
+                @pl.when(inside(z + signs[way]))
+                def _():
+                    line_copy(l, way, 1, kv).start()
+
+            pair_copy(l, 0, 0, kv, c).start()
+
+    def hand_on(l, d):
+        for kv in range(2):
+            for way in range(2):
+
+                @pl.when(inside(z - signs[way] * d))
+                def _():
+                    line_arrival(l, way, d, kv).wait_recv()
+                    if d < n - 1:
+
+                        @pl.when(inside(z + signs[way]))
+                        def _():
+                            line_copy(l, way, d + 1, kv).start()
+
+                    pair_copy(l, way, d, kv, c).start()
+
+    def pair_arrivals(l):
+        for kv in range(2):
+            pair_copy(l, 0, 0, kv, 1 - c).wait_recv()
+            for d in range(1, n):
+                for way in range(2):
+
+                    @pl.when(inside(z - signs[way] * d))
+                    def _():
+                        pair_copy(l, way, d, kv, 1 - c).wait_recv()
+
+    def sends_done(l):
+        for kv in range(2):
+            pair_copy(l, 0, 0, kv, c).wait_send()
+            for d in range(1, n):
+                for way in range(2):
+
+                    @pl.when(jnp.logical_and(inside(z - signs[way] * (d - 1)), inside(z + signs[way])))
+                    def _():
+                        line_copy(l, way, d, kv).wait_send()
+
+                    @pl.when(inside(z - signs[way] * d))
+                    def _():
+                        pair_copy(l, way, d, kv, c).wait_send()
+
+    barrier = pltpu.get_barrier_semaphore()
+    pl.semaphore_signal(barrier, inc=1, device_id={"tp": partner}, device_id_type=mesh_ids)
+    pl.semaphore_signal(barrier, inc=1, device_id={"tp": across}, device_id_type=mesh_ids)
+    for d in range(1, n):
+        pl.semaphore_signal(barrier, inc=1, device_id={"sp": (z + d) % n}, device_id_type=mesh_ids)
+    pl.semaphore_wait(barrier, n + 1)
+    q_share[0].start()
+
+    def normed_rows(values, gain):
+        inverse = lax.rsqrt(jnp.mean(values * values, axis=-1, keepdims=True) + EPSILON)
+        return values * inverse * gain
+
+    def share_normed(l):
+        normed = normed_rows(res[...].astype(f32), query_gain[pl.ds(l, 1), :]).astype(bf16)
+        for j in range(CHUNKS):
+            xb[l, 0, j] = normed[:, j * wide : (j + 1) * wide]
+            gather_copy(l, j).start()
+
+    loads[0].wait()
+    share_normed(0)
+
+    for j in range(CHUNKS):
+        loads[1 + j].wait()
+
+    @pl.loop(0, block // 64)
+    def _(i):
+        part = pl.ds(pl.multiple_of(i * 64, 64), 64)
+        ns[part, :] = normed_rows(raw[part, :].astype(f32), source_gain[...]).astype(bf16)
+
+    for l in range(LAYERS):
+        for copy in kv_loads[l]:
+            copy.wait()
+        made = jnp.dot(ns[...], wkv[l], preferred_element_type=f32).astype(bf16)
+        kh[l, z, c, 0] = made[:, :half]
+        kh[l, z, c, 1] = made[:, half:]
+        if l == 0:
+            send_own(0)
+            o_share[0].start()
+
+    def project_queries(l):
+        q_loads[l].wait()
+        q_share[l].wait_recv()
+        mine = jnp.concatenate([xb[l, 0, j] for j in range(CHUNKS)], axis=1)
+        for slot in range(2):
+            made = jnp.dot(mine, wq[slot, l], preferred_element_type=f32).astype(bf16)
+            for g in range(heads):
+                qs[pl.ds((slot * heads + g) * 2 * rows, rows), :] = made[:, g * HD : (g + 1) * HD]
+        if l == 1:
+            hand_on(1, 2)
+        totals = [None, None]
+        for j in range(CHUNKS):
+            gather_copy(l, j).wait_recv()
+            for slot in range(2):
+                made = jnp.dot(
+                    xb[l, 1, j], wq[slot, l, pl.ds(j * wide, wide), :], preferred_element_type=f32
+                )
+                totals[slot] = made if j == 0 else totals[slot] + made
+        for slot in range(2):
+            made = totals[slot].astype(bf16)
+            for g in range(heads):
+                qs[pl.ds((slot * heads + g) * 2 * rows + rows, rows), :] = made[:, g * HD : (g + 1) * HD]
+
+    def attend_all(l):
+        ms[...] = jnp.full(ms.shape, -1e30, f32)
+        ls[...] = jnp.zeros(ls.shape, f32)
+        acc[...] = jnp.zeros(acc.shape, f32)
+
+        @pl.loop(0, n)
+        def _(s):
+            keys = jnp.concatenate([kh[l, s, 0, 0], kh[l, s, 1, 0]], axis=1)
+            values = jnp.concatenate([kh[l, s, 0, 1], kh[l, s, 1, 1]], axis=1)
+            scores = lax.dot_general(
+                qs[...], keys, (((1,), (1,)), ((), ())), preferred_element_type=f32
+            ) * (HD ** (-0.5))
+            old = ms[...]
+            peak = jnp.maximum(old, jnp.max(scores, axis=1, keepdims=True))
+            weights = jnp.exp(scores - peak)
+            factor = jnp.exp(old - peak)
+            ls[...] = ls[...] * factor + jnp.sum(weights, axis=1, keepdims=True)
+            acc[...] = acc[...] * factor + jnp.dot(
+                weights.astype(bf16), values, preferred_element_type=f32
+            )
+            ms[...] = peak
+
+    for l in range(LAYERS):
+        project_queries(l)
+        if l == 0:
+            hand_on(0, 1)
+            for d in range(2, n):
+                hand_on(0, d)
+                if d == n - 2:
+                    send_own(1)
+        else:
+            for d in range(3, n):
+                hand_on(1, d)
+        pair_arrivals(l)
+        if l == 0:
+            q_share[1].start()
+            o_share[1].start()
+        attend_all(l)
+        out = (acc[...] / ls[...]).astype(bf16)
+        lines = 2 * rows
+        attended = [
+            jnp.concatenate(
+                [out[(slot * heads + g) * lines : (slot * heads + g + 1) * lines] for g in range(heads)], axis=1
+            )
+            for slot in range(2)
+        ]
+        o_loads[l].wait()
+        o_share[l].wait_recv()
+        for j in range(CHUNKS):
+            cut = pl.ds(j * wide, wide)
+            made = jnp.dot(attended[0], wo[0, l, :, cut], preferred_element_type=f32) + jnp.dot(
+                attended[1], wo[1, l, :, cut], preferred_element_type=f32
+            )
+            sb[l, j] = made[rows:].astype(bf16)
+            scatter_copy(l, j).start()
+            pj[:, cut] = made[:rows]
+        if l == 0:
+            hand_on(1, 1)
+        for j in range(CHUNKS):
+            cut = pl.ds(j * wide, wide)
+            scatter_copy(l, j).wait_recv()
+            pj[:, cut] = pj[:, cut] + rb[l, j].astype(f32)
+        res[...] = (
+            res[...].astype(f32) + normed_rows(pj[...], out_gain[pl.ds(l, 1), :])
+        ).astype(bf16)
+        if l + 1 < LAYERS:
+            share_normed(l + 1)
+    result[...] = res[...]
+    for l in range(LAYERS):
+        q_share[l].wait_send()
+        o_share[l].wait_send()
+        for j in range(CHUNKS):
+            gather_copy(l, j).wait_send()
+            scatter_copy(l, j).wait_send()
+        sends_done(l)
+
+
+def fused_body(n, target, source, source_gain, query_gain, out_gain, query_weight, key_weight, value_weight, out_weight):
+    rows, features = target.shape
+    block = source.shape[0]
+    half = key_weight.shape[2]
+    columns = query_weight.shape[2]
+    lines = 2 * rows * 2 * (columns // HD)
+    wide = features // CHUNKS
+    bf16, f32 = jnp.bfloat16, jnp.float32
+    anywhere = pl.BlockSpec(memory_space=pl.ANY)
+    inside = pl.BlockSpec(memory_space=pltpu.VMEM)
+    dma = pltpu.SemaphoreType.DMA
+    line = dma((LAYERS, 2, n, 2))
+    return pl.pallas_call(
+        functools.partial(fused_kernel, n),
+        out_shape=jax.ShapeDtypeStruct(target.shape, bf16),
+        in_specs=[anywhere, anywhere, inside, inside, inside, anywhere, anywhere, anywhere, anywhere],
+        out_specs=inside,
+        scratch_shapes=[
+            pltpu.VMEM((rows, features), bf16),
+            pltpu.VMEM((block, features), bf16),
+            pltpu.VMEM((block, features), bf16),
+            pltpu.VMEM((LAYERS, features, 2 * half), bf16),
+            pltpu.VMEM((2, LAYERS, features, columns), bf16),
+            pltpu.VMEM((2, LAYERS, columns, features), bf16),
+            pltpu.VMEM((LAYERS, n, 2, 2, block, half), bf16),
+            pltpu.VMEM((LAYERS, 2, CHUNKS, rows, wide), bf16),
+            pltpu.VMEM((LAYERS, CHUNKS, rows, wide), bf16),
+            pltpu.VMEM((LAYERS, CHUNKS, rows, wide), bf16),
+            pltpu.VMEM((rows, features), f32),
+            pltpu.VMEM((lines, HD), bf16),
+            pltpu.VMEM((lines, 1), f32),
+            pltpu.VMEM((lines, 1), f32),
+            pltpu.VMEM((lines, HD), f32),
+            dma((1 + CHUNKS,)),
+            dma((LAYERS, 4)),
+            dma((LAYERS, 2)),
+            dma((LAYERS, 2)),
+            dma((LAYERS, CHUNKS)),
+            dma((LAYERS, CHUNKS)),
+            dma((LAYERS, CHUNKS)),
+            dma((LAYERS, CHUNKS)),
+            line,
+            line,
+            line,
+            line,
+        ],
+        compiler_params=pltpu.CompilerParams(
+            collective_id=0, has_side_effects=True, vmem_limit_bytes=60 * 1024 * 1024
+        ),
+    )(
+        target,
+        source,
+        source_gain[None],
+        query_gain,
+        out_gain,
+        query_weight,
+        key_weight,
+        value_weight,
+        out_weight,
+    )
+
+
 def solution(mesh):
     in_specs = (
         P(("grp", "sp", "tp"), None),
@@ -202,4 +607,7 @@
         P(None, "tp", None),
     )
     out_specs = P(("grp", "sp", "tp"), None)
-    return jax.shard_map(body, mesh=mesh, in_specs=in_specs, out_specs=out_specs, check_vma=False)
+    chosen = body
+    if mesh.shape["tp"] == 4 and KVH == 2 and LAYERS == 2 and mesh.shape["sp"] >= 4:
+        chosen = functools.partial(fused_body, mesh.shape["sp"])
+    return jax.shard_map(chosen, mesh=mesh, in_specs=in_specs, out_specs=out_specs, check_vma=False)

time: 190 us -> 70.7 us (0.37)
  waiting for transfers between devices: 105 us -> 0 us
  Pallas kernels: 0 us -> 68.7 us
  blocking collectives: 32.1 us -> 0 us
  matrix products: 16.5 us -> 0 us
  between operations: 15.5 us -> 0.01 us
  other arithmetic: 11.6 us -> 0 us
  local copies, waits for them, and re-layouts: 6.59 us -> 1.67 us
  starting transfers between devices: 2.78 us -> 0 us
    pallas_call x0 -> x1, Pallas kernels: none -> 68.7 us  [fused_body(): pl.pallas_call(functools.partial(fused_kernel, n), out_shape=jax.ShapeDty...]
    all_gather x3 -> x0, waiting for transfers between devices: 52 us -> none  [the longest x2 27 us: body(): lax.all_gather(normed, 'tp', axis=0, tiled=True)]
    reduce_scatter x2 -> x0, waiting for transfers between devices: 49 us -> none  [body(): lax.psum_scatter(jnp.dot(attended, out_layer, preferred_element_type=jnp....]
    all_gather x2 -> x0, blocking collectives: 32.1 us -> none  [the longest x1 16.1 us: body(): lax.all_gather(local_keys[1], 'sp', axis=0, tiled=True)]
    dot_general x9 -> x0, matrix products: 16.5 us -> none  [the longest x2 5.24 us: body(): jnp.dot(lax.all_gather(normed, 'tp', axis=0, tiled=True), layer_weight, p...]
    reduce_sum x7 -> x0, other arithmetic: 6.86 us -> none  [the longest x5 5.04 us: rms_scaled(): jnp.mean(values * values, axis=-1, keepdims=True) + EPSILON]
    convert_element_type x7 -> x0, other arithmetic: 4.48 us -> none  [the longest x2 2.64 us: body(): normed = rms_scaled(residual, query_gain[layer_index]).astype(jnp.bfloat16)]
    ppermute x9 -> x0, waiting for transfers between devices: 3.52 us -> none  [swapped(): return lax.ppermute(value, axis, pairs)]
  transfers between devices with their start and end apart: 14 -> 0, of which waited for: 9 -> 0; matrix products, arithmetic and copies ran while one was open for 6% -> 0% of each run, Pallas kernels for 0% -> 0%
where the time goes in v1:
time: 70.7 us; the launch traced here: 70.4 us
  Pallas kernels  68.7 us (97%)
  local copies, waits for them, and re-layouts  1.67 us (2%)
    pallas_call x1, Pallas kernels, fused_body(): pl.pallas_call(functools.partial(fused_kernel, n), out_shape=jax.ShapeDty...  68.7 us
    unnamed x1, local copies, waits for them, and re-layouts  1.67 us

profile of v1, /device:TPU:0, one launch (start us, length us, event | category | flops | bytes accessed | tf_op | source)
XLA Modules:
  0.0 70.4 jit_solution(12883845372578910785)
XLA Ops:
  0.0 68.7 %shard_map.91 = bf16[64,2048]{1,0:T(8,128)(2,1)} custom-call(bf16[64,2048]{1,0:T(8,128)(2,1)} %target.1, bf16[512,2048]{1,0:T(8,128)(2,1)} %source.1, f32[1,2048]{1,0:T(1,128)} %bitcast.1, f32[2,2048]{1,0:T(2,128)} %query_gain.1, f32[2,2048]{1,0:T(2,128)} %out_gain.1, bf16[2,2048,512]{2,1,0:T(8,128)(2,1)} %query_weight.1, bf16[2,2048,128]{2,1,0:T(8,128)(2,1)} %key_weight.1, ...), custom_call_target="tpu_custom_call" | custom-call | tf_op jit(solution)/shard_map/pallas_call | solution.py:547
  68.8 1.7 %copy.11 = bf16[64,2048]{1,0:T(8,128)(2,1)} copy(bf16[64,2048]{1,0:T(8,128)(2,1)} %shard_map.91) | data formatting | bytes 524288

commit v2 on v1

--- a/solution.py
+++ b/solution.py
@@ -14,6 +14,7 @@
 
 
 EPSILON = 1e-06
+LOG2E = 1.4426950408889634
 
 
 def swapped(value, axis, distance):
@@ -194,6 +195,7 @@
 
 
 CHUNKS = 4
+PARTS = 2
 
 
 def fused_kernel(
@@ -240,7 +242,8 @@
     block = source.shape[0]
     half = key_weight.shape[2]
     wide = target.shape[1] // CHUNKS
-    piece = block // CHUNKS
+    unit = block // PARTS
+    lot = rows // PARTS
     heads = query_weight.shape[2] // HD
     z = lax.axis_index("sp")
     me = lax.axis_index("tp")
@@ -251,9 +254,9 @@
     f32, bf16 = jnp.float32, jnp.bfloat16
 
     loads = [pltpu.make_async_copy(target, res, load_sem.at[0])]
-    for j in range(CHUNKS):
-        part = pl.ds(j * piece, piece)
-        loads.append(pltpu.make_async_copy(source.at[part], raw.at[part], load_sem.at[1 + j]))
+    for u in range(PARTS):
+        part = pl.ds(u * unit, unit)
+        loads.append(pltpu.make_async_copy(source.at[part], raw.at[part], load_sem.at[1 + u]))
     kv_loads, q_loads, o_loads = [], [], []
     for l in range(LAYERS):
         kv_loads.append(
@@ -266,12 +269,8 @@
         o_loads.append(pltpu.make_async_copy(out_weight.at[l], wo.at[0, l], wload_sem.at[l, 3]))
     for copy in loads:
         copy.start()
-    for l in range(LAYERS):
-        for copy in kv_loads[l]:
-            copy.start()
-    for l in range(LAYERS):
-        q_loads[l].start()
-        o_loads[l].start()
+    for copy in kv_loads[0]:
+        copy.start()
 
     def to_partner(src, dst, l, which):
         return pltpu.make_async_remote_copy(
@@ -311,87 +310,87 @@
     def inside(index):
         return jnp.logical_and(index >= 0, index < n)
 
-    def line_copy(l, way, d, kv):
-        ref = kh.at[l, z - signs[way] * (d - 1), c, kv]
+    def line_copy(l, way, d, u):
+        ref = kh.at[l, z - signs[way] * (d - 1), c, u]
         return pltpu.make_async_remote_copy(
             src_ref=ref,
             dst_ref=ref,
-            send_sem=zsend.at[l, way, d, kv],
-            recv_sem=zrecv.at[l, way, d, kv],
+            send_sem=zsend.at[l, way, d, u],
+            recv_sem=zrecv.at[l, way, d, u],
             device_id={"sp": z + signs[way]},
             device_id_type=mesh_ids,
         )
 
-    def line_arrival(l, way, d, kv):
-        ref = kh.at[l, z - signs[way] * d, c, kv]
+    def line_arrival(l, way, d, u):
+        ref = kh.at[l, z - signs[way] * d, c, u]
         return pltpu.make_async_remote_copy(
             src_ref=ref,
             dst_ref=ref,
-            send_sem=zsend.at[l, way, d, kv],
-            recv_sem=zrecv.at[l, way, d, kv],
+            send_sem=zsend.at[l, way, d, u],
+            recv_sem=zrecv.at[l, way, d, u],
             device_id={"sp": z - signs[way]},
             device_id_type=mesh_ids,
         )
 
-    def pair_copy(l, way, d, kv, side):
-        ref = kh.at[l, z - signs[way] * d, side, kv]
+    def pair_copy(l, way, d, u, side):
+        ref = kh.at[l, z - signs[way] * d, side, u]
         return pltpu.make_async_remote_copy(
             src_ref=ref,
             dst_ref=ref,
-            send_sem=psend.at[l, way, d, kv],
-            recv_sem=precv.at[l, way, d, kv],
+            send_sem=psend.at[l, way, d, u],
+            recv_sem=precv.at[l, way, d, u],
             device_id={"tp": partner},
             device_id_type=mesh_ids,
         )
 
-    def send_own(l):
-        for kv in range(2):
-            for way in range(2):
-
-                @pl.when(inside(z + signs[way]))
-                def _():
-                    line_copy(l, way, 1, kv).start()
-
-            pair_copy(l, 0, 0, kv, c).start()
+    def send_own(l, u):
+        for way in range(2):
+
+            @pl.when(inside(z + signs[way]))
+            def _():
+                line_copy(l, way, 1, u).start()
+
+        pair_copy(l, 0, 0, u, c).start()
 
     def hand_on(l, d):
-        for kv in range(2):
+        for u in range(PARTS):
             for way in range(2):
 
                 @pl.when(inside(z - signs[way] * d))
                 def _():
-                    line_arrival(l, way, d, kv).wait_recv()
+                    line_arrival(l, way, d, u).wait_recv()
                     if d < n - 1:
 
                         @pl.when(inside(z + signs[way]))
                         def _():
-                            line_copy(l, way, d + 1, kv).start()
-
-                    pair_copy(l, way, d, kv, c).start()
-
-    def pair_arrivals(l):
-        for kv in range(2):
-            pair_copy(l, 0, 0, kv, 1 - c).wait_recv()
+                            line_copy(l, way, d + 1, u).start()
+
+                    pair_copy(l, way, d, u, c).start()
+
+    def pair_arrivals(l, d):
+        for u in range(PARTS):
+            if d == 0:
+                pair_copy(l, 0, 0, u, 1 - c).wait_recv()
+                continue
+            for way in range(2):
+
+                @pl.when(inside(z - signs[way] * d))
+                def _():
+                    pair_copy(l, way, d, u, 1 - c).wait_recv()
+
+    def sends_done(l):
+        for u in range(PARTS):
+            pair_copy(l, 0, 0, u, c).wait_send()
             for d in range(1, n):
                 for way in range(2):
 
+                    @pl.when(jnp.logical_and(inside(z - signs[way] * (d - 1)), inside(z + signs[way])))
+                    def _():
+                        line_copy(l, way, d, u).wait_send()
+
                     @pl.when(inside(z - signs[way] * d))
                     def _():
-                        pair_copy(l, way, d, kv, 1 - c).wait_recv()
-
-    def sends_done(l):
-        for kv in range(2):
-            pair_copy(l, 0, 0, kv, c).wait_send()
-            for d in range(1, n):
-                for way in range(2):
-
-                    @pl.when(jnp.logical_and(inside(z - signs[way] * (d - 1)), inside(z + signs[way])))
-                    def _():
-                        line_copy(l, way, d, kv).wait_send()
-
-                    @pl.when(inside(z - signs[way] * d))
-                    def _():
-                        pair_copy(l, way, d, kv, c).wait_send()
+                        pair_copy(l, way, d, u, c).wait_send()
 
     barrier = pltpu.get_barrier_semaphore()
     pl.semaphore_signal(barrier, inc=1, device_id={"tp": partner}, device_id_type=mesh_ids)
@@ -399,136 +398,195 @@
     for d in range(1, n):
         pl.semaphore_signal(barrier, inc=1, device_id={"sp": (z + d) % n}, device_id_type=mesh_ids)
     pl.semaphore_wait(barrier, n + 1)
-    q_share[0].start()
-
     def normed_rows(values, gain):
         inverse = lax.rsqrt(jnp.mean(values * values, axis=-1, keepdims=True) + EPSILON)
         return values * inverse * gain
 
-    def share_normed(l):
-        normed = normed_rows(res[...].astype(f32), query_gain[pl.ds(l, 1), :]).astype(bf16)
-        for j in range(CHUNKS):
-            xb[l, 0, j] = normed[:, j * wide : (j + 1) * wide]
-            gather_copy(l, j).start()
+    def share_normed(l, r):
+        part = pl.ds(r * lot, lot)
+        normed = normed_rows(res[part, :].astype(f32), query_gain[pl.ds(l, 1), :])
+        xb[l, 0, r] = normed.astype(bf16)
+        gather_copy(l, r).start()
 
     loads[0].wait()
-    share_normed(0)
-
-    for j in range(CHUNKS):
-        loads[1 + j].wait()
-
-    @pl.loop(0, block // 64)
-    def _(i):
-        part = pl.ds(pl.multiple_of(i * 64, 64), 64)
-        ns[part, :] = normed_rows(raw[part, :].astype(f32), source_gain[...]).astype(bf16)
-
-    for l in range(LAYERS):
-        for copy in kv_loads[l]:
-            copy.wait()
-        made = jnp.dot(ns[...], wkv[l], preferred_element_type=f32).astype(bf16)
-        kh[l, z, c, 0] = made[:, :half]
-        kh[l, z, c, 1] = made[:, half:]
-        if l == 0:
-            send_own(0)
-            o_share[0].start()
-
-    def project_queries(l):
-        q_loads[l].wait()
-        q_share[l].wait_recv()
-        mine = jnp.concatenate([xb[l, 0, j] for j in range(CHUNKS)], axis=1)
+    for r in range(PARTS):
+        share_normed(0, r)
+
+    def make_keys(l, u):
+        made = jnp.dot(ns[pl.ds(u * unit, unit), :], wkv[l], preferred_element_type=f32).astype(bf16)
+        kh[l, z, c, u, 0] = made[:, :half]
+        kh[l, z, c, u, 1] = made[:, half:]
+
+    for u in range(PARTS):
+        loads[1 + u].wait()
+
+        @pl.loop(0, unit // 64)
+        def _(i):
+            part = pl.ds(pl.multiple_of(u * unit + i * 64, 64), 64)
+            ns[part, :] = normed_rows(raw[part, :].astype(f32), source_gain[...]).astype(bf16)
+
+        if u == 0:
+            for copy in kv_loads[0]:
+                copy.wait()
+        make_keys(0, u)
+        send_own(0, u)
+    q_loads[0].start()
+    q_share[0].start()
+    for copy in kv_loads[1]:
+        copy.start()
+    o_loads[0].start()
+    o_share[0].start()
+    q_loads[1].start()
+    o_loads[1].start()
+
+    band = 2 * heads * rows
+
+    def project_queries(l, i):
+        lines = jnp.concatenate([xb[l, i, r] for r in range(PARTS)], axis=0)
         for slot in range(2):
-            made = jnp.dot(mine, wq[slot, l], preferred_element_type=f32).astype(bf16)
+            made = jnp.dot(lines, wq[slot, l], preferred_element_type=f32).astype(bf16)
             for g in range(heads):
-                qs[pl.ds((slot * heads + g) * 2 * rows, rows), :] = made[:, g * HD : (g + 1) * HD]
-        if l == 1:
-            hand_on(1, 2)
-        totals = [None, None]
-        for j in range(CHUNKS):
-            gather_copy(l, j).wait_recv()
-            for slot in range(2):
-                made = jnp.dot(
-                    xb[l, 1, j], wq[slot, l, pl.ds(j * wide, wide), :], preferred_element_type=f32
-                )
-                totals[slot] = made if j == 0 else totals[slot] + made
-        for slot in range(2):
-            made = totals[slot].astype(bf16)
-            for g in range(heads):
-                qs[pl.ds((slot * heads + g) * 2 * rows + rows, rows), :] = made[:, g * HD : (g + 1) * HD]
-
-    def attend_all(l):
-        ms[...] = jnp.full(ms.shape, -1e30, f32)
-        ls[...] = jnp.zeros(ls.shape, f32)
-        acc[...] = jnp.zeros(acc.shape, f32)
-
-        @pl.loop(0, n)
-        def _(s):
-            keys = jnp.concatenate([kh[l, s, 0, 0], kh[l, s, 1, 0]], axis=1)
-            values = jnp.concatenate([kh[l, s, 0, 1], kh[l, s, 1, 1]], axis=1)
-            scores = lax.dot_general(
-                qs[...], keys, (((1,), (1,)), ((), ())), preferred_element_type=f32
-            ) * (HD ** (-0.5))
-            old = ms[...]
-            peak = jnp.maximum(old, jnp.max(scores, axis=1, keepdims=True))
-            weights = jnp.exp(scores - peak)
-            factor = jnp.exp(old - peak)
-            ls[...] = ls[...] * factor + jnp.sum(weights, axis=1, keepdims=True)
-            acc[...] = acc[...] * factor + jnp.dot(
-                weights.astype(bf16), values, preferred_element_type=f32
+                qs[pl.ds(i * band + (slot * heads + g) * rows, rows), :] = made[:, g * HD : (g + 1) * HD]
+
+    def attend(l, s, i, first):
+        def joined(kv):
+            return jnp.concatenate(
+                [jnp.concatenate([kh[l, s, 0, u, kv], kh[l, s, 1, u, kv]], axis=1) for u in range(PARTS)], axis=0
             )
-            ms[...] = peak
-
-    for l in range(LAYERS):
-        project_queries(l)
-        if l == 0:
-            hand_on(0, 1)
-            for d in range(2, n):
-                hand_on(0, d)
-                if d == n - 2:
-                    send_own(1)
+
+        part = pl.ds(i * band, band)
+        scores = lax.dot_general(
+            qs[part, :], joined(0), (((1,), (1,)), ((), ())), preferred_element_type=f32
+        ) * (HD ** (-0.5) * LOG2E)
+        peak = jnp.max(scores, axis=1, keepdims=True)
+        if not first:
+            old = ms[part, :]
+            peak = jnp.maximum(old, peak)
+            factor = jnp.exp2(old - peak)
+        weights = jnp.exp2(scores - peak)
+        sums = weights[:, :128]
+        for k in range(128, block, 128):
+            sums = sums + weights[:, k : k + 128]
+        mixed = jnp.dot(weights.astype(bf16), joined(1), preferred_element_type=f32)
+        ms[part, :] = peak
+        if first:
+            ls[part, :] = sums
+            acc[part, :] = mixed
         else:
-            for d in range(3, n):
-                hand_on(1, d)
-        pair_arrivals(l)
-        if l == 0:
-            q_share[1].start()
-            o_share[1].start()
-        attend_all(l)
-        out = (acc[...] / ls[...]).astype(bf16)
-        lines = 2 * rows
+            ls[part, :] = ls[part, :] * factor + sums
+            acc[part, :] = acc[part, :] * factor + mixed
+
+    def attend_step(l, d, sides):
+        if d == 0:
+            for i in sides:
+                attend(l, z, i, True)
+            return
+
+        @pl.loop(jnp.where(z - d >= 0, 0, 1), jnp.where(z + d < n, 2, 1))
+        def _(way):
+            for i in sides:
+                attend(l, z - (1 - 2 * way) * d, i, False)
+
+    def project_out(l, i):
+        part = pl.ds(i * band, band)
+        out = (acc[part, :] / jnp.sum(ls[part, :], axis=1, keepdims=True)).astype(bf16)
         attended = [
             jnp.concatenate(
-                [out[(slot * heads + g) * lines : (slot * heads + g + 1) * lines] for g in range(heads)], axis=1
+                [out[(slot * heads + g) * rows : (slot * heads + g + 1) * rows] for g in range(heads)], axis=1
             )
             for slot in range(2)
         ]
-        o_loads[l].wait()
-        o_share[l].wait_recv()
         for j in range(CHUNKS):
             cut = pl.ds(j * wide, wide)
             made = jnp.dot(attended[0], wo[0, l, :, cut], preferred_element_type=f32) + jnp.dot(
                 attended[1], wo[1, l, :, cut], preferred_element_type=f32
             )
-            sb[l, j] = made[rows:].astype(bf16)
-            scatter_copy(l, j).start()
-            pj[:, cut] = made[:rows]
-        if l == 0:
-            hand_on(1, 1)
-        for j in range(CHUNKS):
-            cut = pl.ds(j * wide, wide)
-            scatter_copy(l, j).wait_recv()
-            pj[:, cut] = pj[:, cut] + rb[l, j].astype(f32)
-        res[...] = (
-            res[...].astype(f32) + normed_rows(pj[...], out_gain[pl.ds(l, 1), :])
-        ).astype(bf16)
-        if l + 1 < LAYERS:
-            share_normed(l + 1)
+            if i == 0:
+                pj[:, cut] = made
+            else:
+                for r in range(PARTS):
+                    sb[l, r, :, cut] = made[r * lot : (r + 1) * lot].astype(bf16)
+
+    def finish(l, tail):
+        project_out(l, 1)
+        for r in range(PARTS):
+            scatter_copy(l, r).start()
+        tail()
+        project_out(l, 0)
+        for r in range(PARTS):
+            part = pl.ds(r * lot, lot)
+            scatter_copy(l, r).wait_recv()
+            total = pj[part, :] + rb[l, r].astype(f32)
+            res[part, :] = (
+                res[part, :].astype(f32) + normed_rows(total, out_gain[pl.ds(l, 1), :])
+            ).astype(bf16)
+            if l + 1 < LAYERS:
+                share_normed(l + 1, r)
+
+    q_loads[0].wait()
+    q_share[0].wait_recv()
+    project_queries(0, 0)
+    for copy in kv_loads[1]:
+        copy.wait()
+    for u in range(PARTS):
+        make_keys(1, u)
+    for r in range(PARTS):
+        gather_copy(0, r).wait_recv()
+    project_queries(0, 1)
+    for d in range(1, n):
+        hand_on(0, d)
+        if d == n - 2:
+            for u in range(PARTS):
+                send_own(1, u)
+        pair_arrivals(0, d - 1)
+        attend_step(0, d - 1, (1, 0))
+    pair_arrivals(0, n - 1)
+    q_share[1].start()
+    o_share[1].start()
+    attend_step(0, n - 1, (1,))
+    o_loads[0].wait()
+    o_share[0].wait_recv()
+
+    def tail_first():
+        hand_on(1, 1)
+        attend_step(0, n - 1, (0,))
+
+    finish(0, tail_first)
+
+    q_loads[1].wait()
+    q_share[1].wait_recv()
+    hand_on(1, 2)
+    project_queries(1, 0)
+    pair_arrivals(1, 0)
+    attend_step(1, 0, (0,))
+    pair_arrivals(1, 1)
+    attend_step(1, 1, (0,))
+    pair_arrivals(1, 2)
+    attend_step(1, 2, (0,))
+    for d in range(3, n):
+        hand_on(1, d)
+    for r in range(PARTS):
+        gather_copy(1, r).wait_recv()
+    project_queries(1, 1)
+    for d in range(n):
+        if d > 2:
+            pair_arrivals(1, d)
+        attend_step(1, d, (1,))
+    o_loads[1].wait()
+    o_share[1].wait_recv()
+
+    def tail_second():
+        for d in range(3, n):
+            attend_step(1, d, (0,))
+
+    finish(1, tail_second)
     result[...] = res[...]
     for l in range(LAYERS):
         q_share[l].wait_send()
         o_share[l].wait_send()
-        for j in range(CHUNKS):
-            gather_copy(l, j).wait_send()
-            scatter_copy(l, j).wait_send()
+        for r in range(PARTS):
+            gather_copy(l, r).wait_send()
+            scatter_copy(l, r).wait_send()
         sends_done(l)
 
 
@@ -538,12 +596,12 @@
     half = key_weight.shape[2]
     columns = query_weight.shape[2]
     lines = 2 * rows * 2 * (columns // HD)
-    wide = features // CHUNKS
+    lot = rows // PARTS
     bf16, f32 = jnp.bfloat16, jnp.float32
     anywhere = pl.BlockSpec(memory_space=pl.ANY)
     inside = pl.BlockSpec(memory_space=pltpu.VMEM)
     dma = pltpu.SemaphoreType.DMA
-    line = dma((LAYERS, 2, n, 2))
+    line = dma((LAYERS, 2, n, PARTS))
     return pl.pallas_call(
         functools.partial(fused_kernel, n),
         out_shape=jax.ShapeDtypeStruct(target.shape, bf16),
@@ -556,23 +614,23 @@
             pltpu.VMEM((LAYERS, features, 2 * half), bf16),
             pltpu.VMEM((2, LAYERS, features, columns), bf16),
             pltpu.VMEM((2, LAYERS, columns, features), bf16),
-            pltpu.VMEM((LAYERS, n, 2, 2, block, half), bf16),
-            pltpu.VMEM((LAYERS, 2, CHUNKS, rows, wide), bf16),
-            pltpu.VMEM((LAYERS, CHUNKS, rows, wide), bf16),
-            pltpu.VMEM((LAYERS, CHUNKS, rows, wide), bf16),
+            pltpu.VMEM((LAYERS, n, 2, PARTS, 2, block // PARTS, half), bf16),
+            pltpu.VMEM((LAYERS, 2, PARTS, lot, features), bf16),
+            pltpu.VMEM((LAYERS, PARTS, lot, features), bf16),
+            pltpu.VMEM((LAYERS, PARTS, lot, features), bf16),
             pltpu.VMEM((rows, features), f32),
             pltpu.VMEM((lines, HD), bf16),
             pltpu.VMEM((lines, 1), f32),
-            pltpu.VMEM((lines, 1), f32),
+            pltpu.VMEM((lines, 128), f32),
             pltpu.VMEM((lines, HD), f32),
-            dma((1 + CHUNKS,)),
+            dma((1 + PARTS,)),
             dma((LAYERS, 4)),
             dma((LAYERS, 2)),
             dma((LAYERS, 2)),
-            dma((LAYERS, CHUNKS)),
-            dma((LAYERS, CHUNKS)),
-            dma((LAYERS, CHUNKS)),
-            dma((LAYERS, CHUNKS)),
+            dma((LAYERS, PARTS)),
+            dma((LAYERS, PARTS)),
+            dma((LAYERS, PARTS)),
+            dma((LAYERS, PARTS)),
             line,
             line,
             line,

time: 70.7 us -> 61.4 us (0.87)
  Pallas kernels: 68.7 us -> 59.4 us
    pallas_call x1, Pallas kernels: 68.7 us -> 59.4 us  [fused_body(): pl.pallas_call(functools.partial(fused_kernel, n), out_shape=jax.ShapeDty...]
where the time goes in v2:
time: 61.4 us; the launch traced here: 61.1 us
  Pallas kernels  59.4 us (97%)
  local copies, waits for them, and re-layouts  1.67 us (3%)
    pallas_call x1, Pallas kernels, fused_body(): pl.pallas_call(functools.partial(fused_kernel, n), out_shape=jax.ShapeDty...  59.4 us
    unnamed x1, local copies, waits for them, and re-layouts  1.67 us

profile of v2, /device:TPU:0, one launch (start us, length us, event | category | flops | bytes accessed | tf_op | source)
XLA Modules:
  0.0 61.1 jit_solution(12805175692345747878)
XLA Ops:
  0.0 59.4 %shard_map.91 = bf16[64,2048]{1,0:T(8,128)(2,1)} custom-call(bf16[64,2048]{1,0:T(8,128)(2,1)} %target.1, bf16[512,2048]{1,0:T(8,128)(2,1)} %source.1, f32[1,2048]{1,0:T(1,128)} %bitcast.1, f32[2,2048]{1,0:T(2,128)} %query_gain.1, f32[2,2048]{1,0:T(2,128)} %out_gain.1, bf16[2,2048,512]{2,1,0:T(8,128)(2,1)} %query_weight.1, bf16[2,2048,128]{2,1,0:T(8,128)(2,1)} %key_weight.1, ...), custom_call_target="tpu_custom_call" | custom-call | tf_op jit(solution)/shard_map/pallas_call | solution.py:605
  59.4 1.7 %copy.11 = bf16[64,2048]{1,0:T(8,128)(2,1)} copy(bf16[64,2048]{1,0:T(8,128)(2,1)} %shard_map.91) | data formatting | bytes 524288

commit v3 on v2

--- a/solution.py
+++ b/solution.py
@@ -352,8 +352,8 @@
 
         pair_copy(l, 0, 0, u, c).start()
 
-    def hand_on(l, d):
-        for u in range(PARTS):
+    def hand_on(l, d, units=range(PARTS)):
+        for u in units:
             for way in range(2):
 
                 @pl.when(inside(z - signs[way] * d))
@@ -408,10 +408,6 @@
         xb[l, 0, r] = normed.astype(bf16)
         gather_copy(l, r).start()
 
-    loads[0].wait()
-    for r in range(PARTS):
-        share_normed(0, r)
-
     def make_keys(l, u):
         made = jnp.dot(ns[pl.ds(u * unit, unit), :], wkv[l], preferred_element_type=f32).astype(bf16)
         kh[l, z, c, u, 0] = made[:, :half]
@@ -428,12 +424,16 @@
         if u == 0:
             for copy in kv_loads[0]:
                 copy.wait()
+            q_loads[0].start()
+            for copy in kv_loads[1]:
+                copy.start()
         make_keys(0, u)
         send_own(0, u)
-    q_loads[0].start()
+        if u == 0:
+            loads[0].wait()
+            for r in range(PARTS):
+                share_normed(0, r)
     q_share[0].start()
-    for copy in kv_loads[1]:
-        copy.start()
     o_loads[0].start()
     o_share[0].start()
     q_loads[1].start()
@@ -523,23 +523,28 @@
             if l + 1 < LAYERS:
                 share_normed(l + 1, r)
 
-    q_loads[0].wait()
-    q_share[0].wait_recv()
-    project_queries(0, 0)
     for copy in kv_loads[1]:
         copy.wait()
     for u in range(PARTS):
         make_keys(1, u)
+    hand_on(0, 1, (0,))
+    q_loads[0].wait()
+    q_share[0].wait_recv()
+    project_queries(0, 0)
+    hand_on(0, 1, (1,))
     for r in range(PARTS):
         gather_copy(0, r).wait_recv()
     project_queries(0, 1)
-    for d in range(1, n):
-        hand_on(0, d)
+    for d in range(2, n):
+        hand_on(0, d, (0,))
+        pair_arrivals(0, d - 2)
+        attend_step(0, d - 2, (1, 0))
+        hand_on(0, d, (1,))
         if d == n - 2:
             for u in range(PARTS):
                 send_own(1, u)
-        pair_arrivals(0, d - 1)
-        attend_step(0, d - 1, (1, 0))
+    pair_arrivals(0, n - 2)
+    attend_step(0, n - 2, (1, 0))
     pair_arrivals(0, n - 1)
     q_share[1].start()
     o_share[1].start()

time: 61.4 us -> 57.7 us (0.940)
  Pallas kernels: 59.4 us -> 55.8 us
    pallas_call x1, Pallas kernels: 59.4 us -> 55.8 us  [fused_body(): pl.pallas_call(functools.partial(fused_kernel, n), out_shape=jax.ShapeDty...]
where the time goes in v3:
time: 57.7 us; the launch traced here: 57.4 us
  Pallas kernels  55.8 us (97%)
  local copies, waits for them, and re-layouts  1.67 us (3%)
    pallas_call x1, Pallas kernels, fused_body(): pl.pallas_call(functools.partial(fused_kernel, n), out_shape=jax.ShapeDty...  55.8 us
    unnamed x1, local copies, waits for them, and re-layouts  1.67 us

profile of v3, /device:TPU:0, one launch (start us, length us, event | category | flops | bytes accessed | tf_op | source)
XLA Modules:
  0.0 57.4 jit_solution(11972776563045198708)
XLA Ops:
  0.0 55.8 %shard_map.91 = bf16[64,2048]{1,0:T(8,128)(2,1)} custom-call(bf16[64,2048]{1,0:T(8,128)(2,1)} %target.1, bf16[512,2048]{1,0:T(8,128)(2,1)} %source.1, f32[1,2048]{1,0:T(1,128)} %bitcast.1, f32[2,2048]{1,0:T(2,128)} %query_gain.1, f32[2,2048]{1,0:T(2,128)} %out_gain.1, bf16[2,2048,512]{2,1,0:T(8,128)(2,1)} %query_weight.1, bf16[2,2048,128]{2,1,0:T(8,128)(2,1)} %key_weight.1, ...), custom_call_target="tpu_custom_call" | custom-call | tf_op jit(solution)/shard_map/pallas_call | solution.py:610
  55.8 1.7 %copy.11 = bf16[64,2048]{1,0:T(8,128)(2,1)} copy(bf16[64,2048]{1,0:T(8,128)(2,1)} %shard_map.91) | data formatting | bytes 524288
